TPU v7x, 32 devices: a whole 2x2x4 slice. The times are simulated.
32 devices in a mesh: sp: 8 (over z, x), tp: 4 (over y, core).
Axes of the slice: x: 2, y: 2, z: 4, core: 2. Of those that a mesh axis runs over, the one named last changes fastest.
Arguments:
- tokens: bfloat16 [5120, 2048], P(('sp', 'tp')), may hold values from -44 to 44
- in_gain: float32 [2048], replicated, may hold values from 0.1 to 1.9
- w_x: bfloat16 [2048, 2048], P('sp', 'tp'), may hold values from -0.125 to 0.125
- w_z: bfloat16 [2048, 2048], P('sp', 'tp'), may hold values from -0.125 to 0.125
- w_b: bfloat16 [2048, 1024], P('sp', 'tp'), may hold values from -0.125 to 0.125
- w_c: bfloat16 [2048, 1024], P('sp', 'tp'), may hold values from -0.125 to 0.125
- w_dt: bfloat16 [2048, 32], replicated, may hold values from -0.125 to 0.125
- conv_x: float32 [4, 2048], replicated, may hold values from -3 to 3
- conv_b: float32 [4, 1024], replicated, may hold values from -3 to 3
- conv_c: float32 [4, 1024], replicated, may hold values from -3 to 3
- dt_bias: float32 [32], replicated, may hold values from -15 to -3.5
- a_log: float32 [32], replicated, may hold values from -0.5 to 0.5
- out_gain: float32 [2048], replicated, may hold values from 0.1 to 1.9
- w_out: bfloat16 [2048, 2048], P('tp', 'sp'), may hold values from -0.125 to 0.125
Outputs:
- mixer_out: bfloat16 [5120, 2048], P(('sp', 'tp'))
All inputs are finite; a program needn't handle non-finite values.
Results may differ from a plain program's by a relative error of at most 0.015.
Values may be sent and summed in bfloat16 or wider, within the bound.
A program may use at most 128 MiB of HBM per device.

v0:
```python
import jax
import jax.numpy as jnp
from jax import lax
from jax.sharding import PartitionSpec as P

HEAD_DIM = 64
STATE = 128
CONV = 4
BLOCK = 128
EPS = 1e-06
HIGH = lax.Precision.HIGHEST


def carried_in(part, axis, combine, identity):
    place = lax.axis_index(axis)
    gathered = jax.tree.map(lambda a: lax.all_gather(a, axis), part)
    state = jax.tree.map(lambda a, e: jnp.zeros_like(a) + jnp.asarray(e, a.dtype), part, identity)

    def one(lap, state):
        return combine(
            state, jax.tree.map(lambda a: lax.dynamic_index_in_dim(a, lap, 0, False), gathered)
        )

    return lax.fori_loop(0, place, one, state)


def from_behind(value, axis, steps):
    count = lax.axis_size(axis)
    first, last = (max(0, -steps), min(count, count - steps))
    return lax.ppermute(value, axis, [(source, source + steps) for source in range(first, last)])


def inverse_rms(values):
    return lax.rsqrt(jnp.mean(values * values, axis=-1, keepdims=True) + EPS)


def causal_conv(prev_rows, new_rows, kernel):
    joined = jnp.concatenate([prev_rows, new_rows], axis=0).astype(jnp.float32)
    row_count = new_rows.shape[0]
    summed = jnp.zeros(new_rows.shape, jnp.float32)
    for offset in range(kernel.shape[0]):
        summed = summed + kernel[offset] * joined[offset : offset + row_count]
    return jax.nn.silu(summed)


def fold_single(gathered):

    def fold_step(total_part, rows_part, first_row):
        return jnp.dot(gathered, rows_part, preferred_element_type=jnp.float32)

    return fold_step


def fold_products(gathered, totals, weight_rows, first_row):
    single = fold_single(gathered)
    return tuple(
        (
            single(total_part, rows_part, first_row)
            for total_part, rows_part in zip(totals, weight_rows)
        )
    )


def inner_part(cum_decay, b_rows, c_rows, scaled_x, causal):
    scores = jnp.einsum("blgn,bsgn->bgls", c_rows, b_rows, precision=HIGH)
    decay_gap = cum_decay[:, :, None] - cum_decay[:, None, :]
    causal_mask = causal[None, :, :, None, None]
    within = jnp.where(causal_mask, jnp.exp(jnp.where(causal_mask, decay_gap, 0.0)), 0.0)
    return jnp.einsum("bgls,blsgh,bsghp->blghp", scores, within, scaled_x, precision=HIGH)


def carried_part(c_rows, states, cum_decay):
    return jnp.einsum("blgn,bghpn,blgh->blghp", c_rows, states, jnp.exp(cum_decay), precision=HIGH)


def run_blocks(block_states, block_decay, start_state):

    def advance(run_state, inputs):
        fresh_state, factor = inputs
        return (run_state * factor[:, :, None, None] + fresh_state, run_state)

    final_state, entering = lax.scan(advance, start_state, (block_states, block_decay))
    return (entering, final_state)


def chain(earlier, later):
    return (earlier[0] * later[0], earlier[1] * later[0][:, :, None, None] + later[1])


def carry_in(total_decay, final_state):
    identity = (jnp.ones_like(total_decay), jnp.zeros_like(final_state))
    before = carried_in((total_decay, final_state), "sp", chain, identity)
    return before[1]


def body(
    tokens,
    in_gain,
    w_x,
    w_z,
    w_b,
    w_c,
    w_dt,
    conv_x,
    conv_b,
    conv_c,
    dt_bias,
    a_log,
    out_gain,
    w_out,
):
    share_index = lax.axis_index("tp")
    width_x = w_x.shape[1]
    width_b = w_b.shape[1]
    heads_here = width_x // HEAD_DIM
    groups_here = width_b // STATE
    group_heads = heads_here // groups_here
    kernel_x = lax.dynamic_slice_in_dim(conv_x, share_index * width_x, width_x, 1)
    kernel_b = lax.dynamic_slice_in_dim(conv_b, share_index * width_b, width_b, 1)
    kernel_c = lax.dynamic_slice_in_dim(conv_c, share_index * width_b, width_b, 1)
    bias_here = lax.dynamic_slice_in_dim(dt_bias, share_index * heads_here, heads_here, 0)
    rate_here = jnp.exp(lax.dynamic_slice_in_dim(a_log, share_index * heads_here, heads_here, 0))
    gain_here = lax.dynamic_slice_in_dim(out_gain, share_index * width_x, width_x, 0)
    dt_weight = lax.dynamic_slice_in_dim(w_dt, share_index * heads_here, heads_here, 1)
    values = tokens.astype(jnp.float32)
    normed = (values * inverse_rms(values) * in_gain).astype(jnp.bfloat16)
    gathered = lax.all_gather(normed, "tp", axis=0, tiled=True)
    seg_rows = gathered.shape[0]
    blocks = seg_rows // BLOCK
    empty_x = jnp.zeros((seg_rows, width_x), jnp.float32)
    empty_b = jnp.zeros((seg_rows, width_b), jnp.float32)
    projected = fold_products(
        gathered,
        (empty_x, empty_x, empty_b, empty_b),
        (
            lax.all_gather(w_x, "sp", axis=0, tiled=True),
            lax.all_gather(w_z, "sp", axis=0, tiled=True),
            lax.all_gather(w_b, "sp", axis=0, tiled=True),
            lax.all_gather(w_c, "sp", axis=0, tiled=True),
        ),
        jnp.int32(0),
    )
    proj_x, gate_rows, proj_b, proj_c = [
        summed_part.astype(jnp.bfloat16) for summed_part in projected
    ]
    dt_raw = jnp.dot(gathered, dt_weight, preferred_element_type=jnp.float32)
    conv_keep = CONV - 1
    tail_start = seg_rows - conv_keep
    prev_x, prev_b, prev_c = from_behind(
        (proj_x[tail_start:], proj_b[tail_start:], proj_c[tail_start:]), "sp", 1
    )
    conv_xs = causal_conv(prev_x, proj_x, kernel_x)
    conv_bs = causal_conv(prev_b, proj_b, kernel_b)
    conv_cs = causal_conv(prev_c, proj_c, kernel_c)
    step_size = jax.nn.softplus(dt_raw + bias_here)
    log_decay = (-step_size * rate_here).reshape(blocks, BLOCK, groups_here, group_heads)
    causal = lax.broadcasted_iota(jnp.int32, (BLOCK, BLOCK), 0) >= lax.broadcasted_iota(
        jnp.int32, (BLOCK, BLOCK), 1
    )
    cum_decay = jnp.einsum("ls,bsgh->blgh", causal.astype(jnp.float32), log_decay, precision=HIGH)
    scaled_x = (conv_xs.reshape(seg_rows, heads_here, HEAD_DIM) * step_size[:, :, None]).reshape(
        blocks, BLOCK, groups_here, group_heads, HEAD_DIM
    )
    b_rows = conv_bs.reshape(blocks, BLOCK, groups_here, STATE)
    c_rows = conv_cs.reshape(blocks, BLOCK, groups_here, STATE)
    block_total = cum_decay[:, BLOCK - 1]
    tail_weight = jnp.exp(block_total[:, None] - cum_decay)
    block_states = jnp.einsum(
        "blgn,blgh,blghp->bghpn", b_rows, tail_weight, scaled_x, precision=HIGH
    )
    block_decay = jnp.exp(block_total)
    total_decay = jnp.exp(jnp.sum(block_total, axis=0))
    start_state = jnp.zeros(block_states.shape[1:], jnp.float32)
    entering, final_state = run_blocks(block_states, block_decay, start_state)
    incoming = carry_in(total_decay, final_state)

    def per_block(run_state, inputs):
        cum_here, b_here, c_here, x_here, fresh_state, factor = inputs
        output = inner_part(cum_here[None], b_here[None], c_here[None], x_here[None], causal)[0]
        output = output + carried_part(c_here[None], run_state[None], cum_here[None])[0]
        return (run_state * factor[:, :, None, None] + fresh_state, output)

    unused, heads_out = lax.scan(
        per_block, incoming, (cum_decay, b_rows, c_rows, scaled_x, block_states, block_decay)
    )
    gated_out = heads_out.reshape(seg_rows, width_x) * jax.nn.silu(gate_rows.astype(jnp.float32))
    grouped = gated_out.reshape(seg_rows, groups_here, width_x // groups_here)
    mixed_rows = ((grouped * inverse_rms(grouped)).reshape(seg_rows, width_x) * gain_here).astype(
        jnp.bfloat16
    )
    partial_sum = jnp.dot(
        mixed_rows,
        lax.all_gather(w_out, "sp", axis=1, tiled=True),
        preferred_element_type=jnp.float32,
    )
    return lax.psum_scatter(partial_sum.astype(jnp.bfloat16), "tp", scatter_dimension=0, tiled=True)


def solution(mesh):
    in_specs = (
        P(("sp", "tp"), None),
        P(),
        P("sp", "tp"),
        P("sp", "tp"),
        P("sp", "tp"),
        P("sp", "tp"),
        P(),
        P(),
        P(),
        P(),
        P(),
        P(),
        P(),
        P("tp", "sp"),
    )
    out_specs = P(("sp", "tp"), None)
    return jax.shard_map(body, mesh=mesh, in_specs=in_specs, out_specs=out_specs, check_vma=False)
```

profile of v0, /device:TPU:0, one launch (start us, length us, event | category | flops | bytes accessed | tf_op | source)
XLA Modules:
  0.0 366.6 jit_solution(4335275581894576468)
XLA Ops:
  7.9 2.1 fusion.24
  14.8 23.7 %all-gather.11.cloned.1.call-done = bf16[640,2048]{1,0:T(8,128)(2,1)} async-done(((bf16[160,2048]{1,0:T(8,128)(2,1)}), bf16[640,2048]{1,0:T(8,128)(2,1)}) %all-gather.11.cloned.1.call-update) | async-done | bytes 2621456 | tf_op jit(solution)/shard_map/all_gather | solution.py:127
  38.5 2.7 negate_multiply_fusion
  42.1 38.8 %all-gather.15.cloned.1.call-done = bf16[2048,256]{1,0:T(8,128)(2,1)} async-done(((bf16[256,256]{1,0:T(8,128)(2,1)}), bf16[2048,256]{1,0:T(8,128)(2,1)}) %all-gather.15.cloned.1.call-update) | async-done | bytes 1048592 | tf_op jit(solution)/shard_map/all_gather | solution.py:138
  80.9 2.1 convolution_convert_fusion.4
  83.0 2.5 collective-permute-start.1
  85.5 45.4 %all-gather.13.cloned.1.call-done = bf16[2048,512]{1,0:T(8,128)(2,1)} async-done(((bf16[256,512]{1,0:T(8,128)(2,1)}), bf16[2048,512]{1,0:T(8,128)(2,1)}) %all-gather.13.cloned.1.call-update) | async-done | bytes 2097168 | tf_op jit(solution)/shard_map/all_gather | solution.py:136
  130.9 3.1 convolution_convert_fusion.2
  134.8 2.5 collective-permute-start
  151.1 20.7 %all-gather.17.cloned.1.call-done = bf16[2048,256]{1,0:T(8,128)(2,1)} async-done(((bf16[256,256]{1,0:T(8,128)(2,1)}), bf16[2048,256]{1,0:T(8,128)(2,1)}) %all-gather.17.cloned.1.call-update) | async-done | bytes 1048592 | tf_op jit(solution)/shard_map/all_gather | solution.py:139
  171.7 2.9 convolution_convert_fusion.3
  174.6 2.5 collective-permute-start.2
  177.1 17.5 %all-gather.2 = f32[8,2,4]{2,1,0:T(2,128)S(1)} all-gather(f32[1,2,4]{2,1,0:T(2,128)S(1)} %exponential_bitcast_fusion.1), channel_id=2, replica_groups=mesh['sp'=8,'tp'=4] {'sp'}, dimensions={0}, use_global_device_ids=true | all-gather | bytes 288 | tf_op jit(solution)/shard_map/all_gather | solution.py:16
  197.4 24.2 %all-gather.23.cloned.1.call-done = f32[16,4,64,128]{3,2,1,0:T(8,128)} async-done(((f32[2,4,64,128]{3,2,1,0:T(8,128)}), f32[16,4,64,128]{3,2,1,0:T(8,128)}) %all-gather.23.cloned.1.call-update) | async-done | bytes 2097168 | tf_op jit(solution)/shard_map/all_gather | solution.py:16
  221.8 24.1 %while.38 = (s32[]{:T(128)}, f32[2,4,64,128]{3,2,1,0:T(8,128)S(1)}, f32[5,128,2,4,64]{1,4,3,2,0:T(8,128)}, f32[5,2,4]{2,1,0:T(2,128)S(1)}, f32[5,2,4,64,128]{4,3...) while((s32[]{:T(128)}, f32[2,4,64,128]{3,2,1,0:T(8,128)S(1)}, ...), condition=%wide.region_7.8_spmd.clone.clone, body=%wide.region_6.7_spmd.clone.clone.sunk | while | flops 252461056 | bytes 3863257 | solution.py:183
  222.7 1.9 constant_dynamic-slice_fusion.13
  224.5 1.9 fusion.77
  227.5 1.9 constant_dynamic-slice_fusion.13
  229.4 1.9 fusion.77
  232.3 1.9 constant_dynamic-slice_fusion.13
  234.2 1.9 fusion.77
  237.1 1.9 constant_dynamic-slice_fusion.13
  239.0 1.9 fusion.77
  241.9 1.9 constant_dynamic-slice_fusion.13
  243.8 1.9 fusion.77
  245.9 3.0 copy.89
  248.9 2.8 reshape.123
  251.7 19.6 %all-gather.19.cloned.1.call-done = bf16[2048,512]{1,0:T(8,128)(2,1)} async-done(((bf16[256,512]{1,0:T(8,128)(2,1)}), bf16[2048,512]{1,0:T(8,128)(2,1)}) %all-gather.19.cloned.1.call-update) | async-done | bytes 2097168 | tf_op jit(solution)/shard_map/all_gather | solution.py:137
  271.3 5.5 %fusion.49 = (f32[640,512]{1,0:T(8,128)S(1)}, f32[640,512]{1,0:T(8,128)}) fusion(f32[640,512]{1,0:T(8,128)} %reshape.123, bf16[640,2048]{1,0:T(8,128)(2,1)} %all-gather.11.cloned.1.call-done, bf16[2048,512]{1,0:T(8,128)(2,1)} %all-gather.19.cloned.1.call-done), kind=kOutput, calls=%fused_computation.107 | convolution fusion | flops 1344798720 | bytes 8650752 | tf_op jit(solution)/shard_map/dot_general | solution.py:49
  279.5 42.8 %all-gather.21.cloned.1.call-done = bf16[512,2048]{1,0:T(8,128)(2,1)} async-done(((bf16[512,256]{1,0:T(8,128)(2,1)}), bf16[512,2048]{1,0:T(8,128)(2,1)}) %all-gather.21.cloned.1.call-update) | async-done | bytes 2097168 | tf_op jit(solution)/shard_map/all_gather | solution.py:193
  322.3 4.6 %convolution_convert_fusion = bf16[640,2048]{1,0:T(8,128)(2,1)} fusion(bf16[512,2048]{1,0:T(8,128)(2,1)} %all-gather.21.cloned.1.call-done, f32[640,512]{1,0:T(8,128)S(1)} %copy-done.11, f32[640,512]{1,0:T(8,128)S(1)} %bitcast.131, f32[512]{0:T(512)S(1)} %dynamic_slice.66), kind=kOutput, calls=%fused_computation.38 | convolution fusion | flops 1344471040 | bytes 7342080 | tf_op jit(solution)/shard_map/dot_general | solution.py:191
  326.9 32.8 %reduce-scatter.2.cloned.1.call-done = bf16[160,2048]{1,0:T(8,128)(2,1)} async-done(((bf16[640,2048]{1,0:T(8,128)(2,1)}), bf16[160,2048]{1,0:T(8,128)(2,1)}) %reduce-scatter.2.cloned.1.call-update) | async-done | bytes 655376 | tf_op jit(solution)/shard_map/reduce_scatter | solution.py:196
  (133 shorter events, 32.2 us)
Async XLA Ops:
  6.5 32.0 %copy-start = (bf16[2048,32]{0,1:T(8,128)(2,1)S(1)}, bf16[2048,32]{0,1:T(8,128)(2,1)}, u32[]{:S(2)}) copy-start(bf16[2048,32]{0,1:T(8,128)(2,1)} %param.26) | copy-start | bytes 393220
  6.5 32.0 %all-gather.11.cloned.1.call-start = ((), (), s32[]{:S(2)}) async-start(), calls=%async_computation.1 | async-start | bytes 3276800 | tf_op jit(solution)/shard_map/all_gather | solution.py:127
  7.9 4.3 %copy-start.9 = (f32[32]{0:T(128)S(1)}, f32[32]{0:T(128)}, u32[]{:S(2)}) copy-start(f32[32]{0:T(128)} %param.31) | copy-start | bytes 388
  7.9 4.4 %copy-start.10 = (f32[32]{0:T(128)S(1)}, f32[32]{0:T(128)}, u32[]{:S(2)}) copy-start(f32[32]{0:T(128)} %param.30) | copy-start | bytes 388
  10.1 70.8 %all-gather.15.cloned.1.call-start = ((), (), s32[]{:S(2)}) async-start(), calls=%async_computation.3 | async-start | bytes 1179648 | tf_op jit(solution)/shard_map/all_gather | solution.py:138
  10.8 120.1 %all-gather.13.cloned.1.call-start = ((), (), s32[]{:S(2)}) async-start(), calls=%async_computation.2 | async-start | bytes 2359296 | tf_op jit(solution)/shard_map/all_gather | solution.py:136
  11.6 160.2 %all-gather.17.cloned.1.call-start = ((), (), s32[]{:S(2)}) async-start(), calls=%async_computation.4 | async-start | bytes 1179648 | tf_op jit(solution)/shard_map/all_gather | solution.py:139
  12.1 209.4 %all-gather.23.cloned.1.call-start = ((), (), s32[]{:S(2)}) async-start(), calls=%async_computation.8 | async-start | bytes 2359296 | tf_op jit(solution)/shard_map/all_gather | solution.py:16
  38.5 42.4 %copy-start.2 = (bf16[640,2048]{1,0:T(8,128)(2,1)S(1)}, bf16[640,2048]{1,0:T(8,128)(2,1)}, u32[]{:S(2)}) copy-start(bf16[640,2048]{1,0:T(8,128)(2,1)} %all-gather.11.cloned.1.call-done) | copy-start | bytes 7864324
  83.0 55.0 %collective-permute-start.1 = (bf16[3,256]{1,0:T(4,128)(2,1)S(1)}, bf16[3,256]{1,0:T(4,128)(2,1)S(1)}, u32[]{:S(2)}, u32[]{:S(2)}) collective-permute-start(bf16[3,256]{1,0:T(4,128)(2,1)S(1)} %slice.118), channel_id=1, source_target_pairs={{0,4},{4,8},{8,12},{12,16},{16,20},{20,24},{24,28},{1,5},{5,9},{9,... | collective-permute-start | bytes 4616 | tf_op jit(solution)/shard_map/ppermute | solution.py:30
  134.0 0.8 copy-start.3
  134.8 4.0 %collective-permute-start = (bf16[3,512]{1,0:T(4,128)(2,1)S(1)}, bf16[3,512]{1,0:T(4,128)(2,1)S(1)}, u32[]{:S(2)}, u32[]{:S(2)}) collective-permute-start(bf16[3,512]{1,0:T(4,128)(2,1)S(1)} %slice.113), channel_id=1, source_target_pairs={{0,4},{4,8},{8,12},{12,16},{16,20},{20,24},{24,28},{1,5},{5,9},{9,... | collective-permute-start | bytes 9224 | tf_op jit(solution)/shard_map/ppermute | solution.py:30
  138.5 1.1 copy-start.4
  138.8 0.9 copy-start.6
  138.9 0.9 copy-start.7
  142.1 1.4 copy-start.5
  147.3 0.7 copy-start.1
  148.0 123.3 %all-gather.19.cloned.1.call-start = ((), (), s32[]{:S(2)}) async-start(), calls=%async_computation.5 | async-start | bytes 2359296 | tf_op jit(solution)/shard_map/all_gather | solution.py:137
  148.6 173.7 %all-gather.21.cloned.1.call-start = ((), (), s32[]{:S(2)}) async-start(), calls=%async_computation.6 | async-start | bytes 2359296 | tf_op jit(solution)/shard_map/all_gather | solution.py:193
  149.3 210.4 %reduce-scatter.2.cloned.1.call-start = ((), (), s32[]{:S(2)}) async-start(), calls=%async_computation.7 | async-start | bytes 3276800 | tf_op jit(solution)/shard_map/reduce_scatter | solution.py:196
  151.1 26.0 %copy-start.8 = (f32[2,4]{1,0:T(2,128)S(1)}, f32[2,4]{1,0:T(2,128)}, u32[]{:S(2)}) copy-start(f32[2,4]{1,0:T(2,128)} %get-tuple-element.254) | copy-start | bytes 100
  174.6 20.1 %collective-permute-start.2 = (bf16[3,256]{1,0:T(4,128)(2,1)S(1)}, bf16[3,256]{1,0:T(4,128)(2,1)S(1)}, u32[]{:S(2)}, u32[]{:S(2)}) collective-permute-start(bf16[3,256]{1,0:T(4,128)(2,1)S(1)} %slice.123), channel_id=1, source_target_pairs={{0,4},{4,8},{8,12},{12,16},{16,20},{20,24},{24,28},{1,5},{5,9},{9,... | collective-permute-start | bytes 4616 | tf_op jit(solution)/shard_map/ppermute | solution.py:30
  279.4 42.9 %copy-start.11 = (f32[640,512]{1,0:T(8,128)S(1)}, f32[640,512]{1,0:T(8,128)}, u32[]{:S(2)}) copy-start(f32[640,512]{1,0:T(8,128)} %get-tuple-element.310) | copy-start | bytes 3932164
Sparse Core Ops, SparseCore 0:
  10.2 28.2 all-gather.10
  40.6 40.2 all-gather.14
  83.0 47.7 all-gather.12
  132.9 38.8 all-gather.16
  173.7 47.8 all-gather.22
  223.5 47.7 all-gather.18
  273.3 48.8 all-gather.20
  327.0 32.6 reduce-scatter.1
where the time goes:
time: 368 us; the launch traced here: 367 us
  waiting for transfers between devices  251 us (68%)
  matrix products  36 us (10%)
  local copies, waits for them, and re-layouts  29 us (8%)
  blocking collectives  17.5 us (5%)
  between operations  13.9 us (4%)
  other arithmetic  10.7 us (3%)
  starting transfers between devices  7.7 us (2%)
    all_gather x1, waiting for transfers between devices, body(): lax.all_gather(w_x, 'sp', axis=0, tiled=True)  45.4 us
    all_gather x1, waiting for transfers between devices, body(): lax.all_gather(w_out, 'sp', axis=1, tiled=True)  42.8 us
    all_gather x1, waiting for transfers between devices, body(): lax.all_gather(w_b, 'sp', axis=0, tiled=True)  38.8 us
    reduce_scatter x1, waiting for transfers between devices, body(): lax.psum_scatter(partial_sum.astype(jnp.bfloat16), 'tp', scatter_dimensio...  32.8 us
    all_gather x1, waiting for transfers between devices, carried_in(): gathered = jax.tree.map(lambda a: lax.all_gather(a, axis), part)  24.2 us
    all_gather x1, waiting for transfers between devices, body(): gathered = lax.all_gather(normed, 'tp', axis=0, tiled=True)  23.7 us
    all_gather x1, waiting for transfers between devices, body(): lax.all_gather(w_c, 'sp', axis=0, tiled=True)  20.7 us
    all_gather x1, waiting for transfers between devices, body(): lax.all_gather(w_z, 'sp', axis=0, tiled=True)  19.6 us
  transfers between devices with their start and end apart: 11, of which 8 were waited for; matrix products, arithmetic and copies ran while one was open for 18% of the time, Pallas kernels for 0%

commit v1 on v0

--- a/solution.py
+++ b/solution.py
@@ -124,7 +124,12 @@
     dt_weight = lax.dynamic_slice_in_dim(w_dt, share_index * heads_here, heads_here, 1)
     values = tokens.astype(jnp.float32)
     normed = (values * inverse_rms(values) * in_gain).astype(jnp.bfloat16)
-    gathered = lax.all_gather(normed, "tp", axis=0, tiled=True)
+    ring = [normed]
+    for hop in range(3):
+        ring.append(lax.ppermute(ring[-1], "tp", [(dev, (dev + 1) % 4) for dev in range(4)]))
+    gathered = jnp.roll(
+        jnp.concatenate(ring[::-1], axis=0), (lax.axis_index("tp") + 1) * ring[0].shape[0], axis=0
+    )
     seg_rows = gathered.shape[0]
     blocks = seg_rows // BLOCK
     empty_x = jnp.zeros((seg_rows, width_x), jnp.float32)

time: 368 us -> 339 us (0.921)
  waiting for transfers between devices: 251 us -> 216 us
    all_gather x1, waiting for transfers between devices: 38.8 us -> 3.88 us  [body(): lax.all_gather(w_b, 'sp', axis=0, tiled=True)]
    ppermute x0 -> x3, waiting for transfers between devices: none -> 28.1 us  [body(): lax.ppermute(ring[-1], 'tp', [(dev, (dev + 1) % 4) for dev in range(4)])]
    all_gather x1 -> x0, waiting for transfers between devices: 23.7 us -> none  [body(): gathered = lax.all_gather(normed, 'tp', axis=0, tiled=True)]
    all_gather x1, waiting for transfers between devices: 45.4 us -> 41.3 us  [body(): lax.all_gather(w_x, 'sp', axis=0, tiled=True)]
    unnamed x27 -> x23, local copies, waits for them, and re-layouts: 2.37 us -> 6.3 us
  transfers between devices with their start and end apart: 11 -> 13, of which waited for: 8 -> 11; matrix products, arithmetic and copies ran while one was open for 18% -> 23% of each run, Pallas kernels for 0% -> 0%
where the time goes in v1:
time: 339 us; the launch traced here: 338 us
  waiting for transfers between devices  216 us (64%)
  matrix products  37.6 us (11%)
  local copies, waits for them, and re-layouts  31.1 us (9%)
  blocking collectives  17.5 us (5%)
  between operations  13.8 us (4%)
  other arithmetic  13 us (4%)
  starting transfers between devices  8.23 us (2%)
    all_gather x1, waiting for transfers between devices, body(): lax.all_gather(w_out, 'sp', axis=1, tiled=True)  42.6 us
    all_gather x1, waiting for transfers between devices, body(): lax.all_gather(w_x, 'sp', axis=0, tiled=True)  41.3 us
    reduce_scatter x1, waiting for transfers between devices, body(): lax.psum_scatter(partial_sum.astype(jnp.bfloat16), 'tp', scatter_dimensio...  32.8 us
    ppermute x3, waiting for transfers between devices, body(): lax.ppermute(ring[-1], 'tp', [(dev, (dev + 1) % 4) for dev in range(4)])  28.1 us
    all_gather x1, waiting for transfers between devices, carried_in(): gathered = jax.tree.map(lambda a: lax.all_gather(a, axis), part)  26.1 us
    all_gather x1, waiting for transfers between devices, body(): lax.all_gather(w_z, 'sp', axis=0, tiled=True)  19.6 us
    all_gather x1, waiting for transfers between devices, body(): lax.all_gather(w_c, 'sp', axis=0, tiled=True)  18.7 us
    all_gather x1, blocking collectives, carried_in(): gathered = jax.tree.map(lambda a: lax.all_gather(a, axis), part)  17.5 us
  transfers between devices with their start and end apart: 13, of which 11 were waited for; matrix products, arithmetic and copies ran while one was open for 23% of the time, Pallas kernels for 0%

profile of v1, /device:TPU:0, one launch (start us, length us, event | category | flops | bytes accessed | tf_op | source)
XLA Modules:
  0.0 338.2 jit_solution(3468025172702865657)
XLA Ops:
  10.8 10.2 %collective-permute-done = bf16[160,2048]{1,0:T(8,128)(2,1)S(1)} collective-permute-done((bf16[160,2048]{1,0:T(8,128)(2,1)S(1)}, bf16[160,2048]{1,0:T(8,128)(2,1)S(1)}, u32[]{:S(2)}, u32[]{:S(2)}) %collective-permute-start) | collective-permute-done | bytes 655392 | tf_op jit(solution)/shard_map/ppermute | solution.py:129
  21.1 10.0 %collective-permute-done.1 = bf16[160,2048]{1,0:T(8,128)(2,1)S(1)} collective-permute-done((bf16[160,2048]{1,0:T(8,128)(2,1)S(1)}, bf16[160,2048]{1,0:T(8,128)(2,1)S(1)}, u32[]{:S(2)}, u32[]{:S(2)}) %collective-permute-start.1) | collective-permute-done | bytes 655392 | tf_op jit(solution)/shard_map/ppermute | solution.py:129
  33.2 7.9 %collective-permute-done.2 = bf16[160,2048]{1,0:T(8,128)(2,1)S(1)} collective-permute-done((bf16[160,2048]{1,0:T(8,128)(2,1)S(1)}, bf16[160,2048]{1,0:T(8,128)(2,1)S(1)}, u32[]{:S(2)}, u32[]{:S(2)}) %collective-permute-start.2) | collective-permute-done | bytes 655392 | tf_op jit(solution)/shard_map/ppermute | solution.py:129
  48.6 3.9 %all-gather.12.cloned.1.call-done = bf16[2048,256]{1,0:T(8,128)(2,1)} async-done(((bf16[256,256]{1,0:T(8,128)(2,1)}), bf16[2048,256]{1,0:T(8,128)(2,1)}) %all-gather.12.cloned.1.call-update) | async-done | bytes 1048592 | tf_op jit(solution)/shard_map/all_gather | solution.py:143
  52.5 2.9 fusion.50
  55.4 2.5 collective-permute-start.4
  57.9 2.6 negate_multiply_fusion
  61.2 41.3 %all-gather.10.cloned.1.call-done = bf16[2048,512]{1,0:T(8,128)(2,1)} async-done(((bf16[256,512]{1,0:T(8,128)(2,1)}), bf16[2048,512]{1,0:T(8,128)(2,1)}) %all-gather.10.cloned.1.call-update) | async-done | bytes 2097168 | tf_op jit(solution)/shard_map/all_gather | solution.py:141
  102.5 3.9 %fusion.32 = bf16[640,512]{1,0:T(8,128)(2,1)S(1)} fusion(bf16[2048,512]{1,0:T(8,128)(2,1)} %all-gather.10.cloned.1.call-done, bf16[1280,2048]{1,0:T(8,128)(2,1)} %constant_dynamic-update-slice_fusion, s32[]{:T(128)S(6)} %select_n.51), kind=kOutput, calls=%fused_computation.53 | convolution fusion | flops 1342504960 | bytes 5373956 | tf_op jit(solution)/shard_map/dot_general | solution.py:49
  106.4 2.4 collective-permute-start.3
  115.5 3.5 %broadcast_multiply_fusion.1 = (f32[5,128,2,4,64]{1,0,4,3,2:T(8,128)S(1)}, f32[5,128,2,4,64]{1,0,4,3,2:T(8,128)}) fusion(f32[5,128,2,4]{1,0,3,2:T(8,128)S(1)} %subtract_exponential_fusion, f32[5,128,2,4,64]{1,0,4,3,2:T(8,128)} %reshape.103, f32[5,128,2,4]{1,0,3,2:T(8,128)S(1)} %copy.69), kind=kLoop, calls=%fused_computation.78 | loop fusion | flops 655360 | bytes 3973120 | tf_op jit(solution)/shard_map/blgn,blgh,blghp->bghpn/dot_general | solution.py:173
  124.7 18.7 %all-gather.14.cloned.1.call-done = bf16[2048,256]{1,0:T(8,128)(2,1)} async-done(((bf16[256,256]{1,0:T(8,128)(2,1)}), bf16[2048,256]{1,0:T(8,128)(2,1)}) %all-gather.14.cloned.1.call-update) | async-done | bytes 1048592 | tf_op jit(solution)/shard_map/all_gather | solution.py:144
  143.4 2.9 fusion.53
  146.3 2.5 collective-permute-start.5
  148.8 17.5 %all-gather.2 = f32[8,2,4]{2,1,0:T(2,128)S(1)} all-gather(f32[1,2,4]{2,1,0:T(2,128)S(1)} %exponential_bitcast_fusion.1), channel_id=2, replica_groups=mesh['sp'=8,'tp'=4] {'sp'}, dimensions={0}, use_global_device_ids=true | all-gather | bytes 288 | tf_op jit(solution)/shard_map/all_gather | solution.py:16
  167.2 26.1 %all-gather.20.cloned.1.call-done = f32[16,4,64,128]{3,2,1,0:T(8,128)} async-done(((f32[2,4,64,128]{3,2,1,0:T(8,128)}), f32[16,4,64,128]{3,2,1,0:T(8,128)}) %all-gather.20.cloned.1.call-update) | async-done | bytes 2097168 | tf_op jit(solution)/shard_map/all_gather | solution.py:16
  193.5 24.1 %while.38 = (s32[]{:T(128)}, f32[2,4,64,128]{3,2,1,0:T(8,128)S(1)}, f32[5,128,2,4,64]{1,4,3,2,0:T(8,128)}, f32[5,2,4]{2,1,0:T(2,128)S(1)}, f32[5,2,4,64,128]{4,3...) while((s32[]{:T(128)}, f32[2,4,64,128]{3,2,1,0:T(8,128)S(1)}, ...), condition=%wide.region_7.8_spmd.clone.clone, body=%wide.region_6.7_spmd.clone.clone.sunk | while | flops 252461056 | bytes 3863257 | solution.py:188
  194.4 1.9 constant_dynamic-slice_fusion.13
  196.3 1.9 fusion.105
  199.2 1.9 constant_dynamic-slice_fusion.13
  201.1 1.9 fusion.105
  204.0 1.9 constant_dynamic-slice_fusion.13
  205.9 1.9 fusion.105
  210.7 2.0 fusion.105
  215.6 2.0 fusion.105
  217.6 3.0 copy.89
  220.7 2.7 reshape.123
  223.4 19.6 %all-gather.16.cloned.1.call-done = bf16[2048,512]{1,0:T(8,128)(2,1)} async-done(((bf16[256,512]{1,0:T(8,128)(2,1)}), bf16[2048,512]{1,0:T(8,128)(2,1)}) %all-gather.16.cloned.1.call-update) | async-done | bytes 2097168 | tf_op jit(solution)/shard_map/all_gather | solution.py:142
  243.0 5.6 %fusion.82 = (f32[640,512]{1,0:T(8,128)S(1)}, f32[640,512]{1,0:T(8,128)}) fusion(f32[640,512]{1,0:T(8,128)} %reshape.123, bf16[2048,512]{1,0:T(8,128)(2,1)} %all-gather.16.cloned.1.call-done, bf16[1280,2048]{1,0:T(8,128)(2,1)} %constant_dynamic-update-slice_fusion, s32[]{:T(128)S(6)} %select_n.51), kind=kOutput, calls=%fused_computation.129 | convolution fusion | flops 1344798720 | bytes 8650756 | tf_op jit(solution)/shard_map/dot_general | solution.py:49
  251.2 42.6 %all-gather.18.cloned.1.call-done = bf16[512,2048]{1,0:T(8,128)(2,1)} async-done(((bf16[512,256]{1,0:T(8,128)(2,1)}), bf16[512,2048]{1,0:T(8,128)(2,1)}) %all-gather.18.cloned.1.call-update) | async-done | bytes 2097168 | tf_op jit(solution)/shard_map/all_gather | solution.py:198
  293.8 4.6 %convolution_convert_fusion = bf16[640,2048]{1,0:T(8,128)(2,1)} fusion(bf16[512,2048]{1,0:T(8,128)(2,1)} %all-gather.18.cloned.1.call-done, f32[640,512]{1,0:T(8,128)S(1)} %copy-done.6, f32[640,512]{1,0:T(8,128)S(1)} %bitcast.126, f32[512]{0:T(512)S(1)} %dynamic_slice.71), kind=kOutput, calls=%fused_computation.38 | convolution fusion | flops 1344471040 | bytes 7342080 | tf_op jit(solution)/shard_map/dot_general | solution.py:196
  298.5 32.8 %reduce-scatter.2.cloned.1.call-done = bf16[160,2048]{1,0:T(8,128)(2,1)} async-done(((bf16[640,2048]{1,0:T(8,128)(2,1)}), bf16[160,2048]{1,0:T(8,128)(2,1)}) %reduce-scatter.2.cloned.1.call-update) | async-done | bytes 655376 | tf_op jit(solution)/shard_map/reduce_scatter | solution.py:201
  (134 shorter events, 39.4 us)
Async XLA Ops:
  6.5 51.4 %copy-start = (bf16[2048,32]{0,1:T(8,128)(2,1)S(1)}, bf16[2048,32]{0,1:T(8,128)(2,1)}, u32[]{:S(2)}) copy-start(bf16[2048,32]{0,1:T(8,128)(2,1)} %param.26) | copy-start | bytes 393220
  6.5 2.8 copy-start.1
  6.5 24.7 %copy-start.4 = (f32[32]{0:T(128)S(1)}, f32[32]{0:T(128)}, u32[]{:S(2)}) copy-start(f32[32]{0:T(128)} %param.30) | copy-start | bytes 388
  6.5 24.7 %copy-start.5 = (f32[32]{0:T(128)S(1)}, f32[32]{0:T(128)}, u32[]{:S(2)}) copy-start(f32[32]{0:T(128)} %param.31) | copy-start | bytes 388
  6.5 46.0 %all-gather.12.cloned.1.call-start = ((), (), s32[]{:S(2)}) async-start(), calls=%async_computation.2 | async-start | bytes 1179648 | tf_op jit(solution)/shard_map/all_gather | solution.py:143
  7.3 95.2 %all-gather.10.cloned.1.call-start = ((), (), s32[]{:S(2)}) async-start(), calls=%async_computation.1 | async-start | bytes 2359296 | tf_op jit(solution)/shard_map/all_gather | solution.py:141
  8.0 135.4 %all-gather.14.cloned.1.call-start = ((), (), s32[]{:S(2)}) async-start(), calls=%async_computation.3 | async-start | bytes 1179648 | tf_op jit(solution)/shard_map/all_gather | solution.py:144
  10.3 10.8 %collective-permute-start = (bf16[160,2048]{1,0:T(8,128)(2,1)S(1)}, bf16[160,2048]{1,0:T(8,128)(2,1)S(1)}, u32[]{:S(2)}, u32[]{:S(2)}) collective-permute-start(bf16[160,2048]{1,0:T(8,128)(2,1)S(1)} %fusion.40), channel_id=1, source_target_pairs={{0,1},{1,2},{2,3},{3,0},{4,5},{5,6},{6,7},{7,4},{8,9},{9,10},{10,1... | collective-permute-start | bytes 1966088 | tf_op jit(solution)/shard_map/ppermute | solution.py:129
  21.1 10.0 %collective-permute-start.1 = (bf16[160,2048]{1,0:T(8,128)(2,1)S(1)}, bf16[160,2048]{1,0:T(8,128)(2,1)S(1)}, u32[]{:S(2)}, u32[]{:S(2)}) collective-permute-start(bf16[160,2048]{1,0:T(8,128)(2,1)S(1)} %collective-permute-done), channel_id=1, source_target_pairs={{0,1},{1,2},{2,3},{3,0},{4,5},{5,6},{6,7},{7,4},{8,9},{9,10},{10,1... | collective-permute-start | bytes 1966088 | tf_op jit(solution)/shard_map/ppermute | solution.py:129
  31.1 10.0 %collective-permute-start.2 = (bf16[160,2048]{1,0:T(8,128)(2,1)S(1)}, bf16[160,2048]{1,0:T(8,128)(2,1)S(1)}, u32[]{:S(2)}, u32[]{:S(2)}) collective-permute-start(bf16[160,2048]{1,0:T(8,128)(2,1)S(1)} %collective-permute-done.1), channel_id=1, source_target_pairs={{0,1},{1,2},{2,3},{3,0},{4,5},{5,6},{6,7},{7,4},{8,9},{9,10},{10,1... | collective-permute-start | bytes 1966088 | tf_op jit(solution)/shard_map/ppermute | solution.py:129
  31.1 162.2 %all-gather.20.cloned.1.call-start = ((), (), s32[]{:S(2)}) async-start(), calls=%async_computation.7 | async-start | bytes 2359296 | tf_op jit(solution)/shard_map/all_gather | solution.py:16
  42.0 1.8 copy-start.3
  55.4 5.7 %collective-permute-start.4 = (bf16[3,256]{1,0:T(4,128)(2,1)S(1)}, bf16[3,256]{1,0:T(4,128)(2,1)S(1)}, u32[]{:S(2)}, u32[]{:S(2)}) collective-permute-start(bf16[3,256]{1,0:T(4,128)(2,1)S(1)} %slice.118), channel_id=1, source_target_pairs={{0,4},{4,8},{8,12},{12,16},{16,20},{20,24},{24,28},{1,5},{5,9},{9,... | collective-permute-start | bytes 4616 | tf_op jit(solution)/shard_map/ppermute | solution.py:30
  106.4 3.8 %collective-permute-start.3 = (bf16[3,512]{1,0:T(4,128)(2,1)S(1)}, bf16[3,512]{1,0:T(4,128)(2,1)S(1)}, u32[]{:S(2)}, u32[]{:S(2)}) collective-permute-start(bf16[3,512]{1,0:T(4,128)(2,1)S(1)} %slice.113), channel_id=1, source_target_pairs={{0,4},{4,8},{8,12},{12,16},{16,20},{20,24},{24,28},{1,5},{5,9},{9,... | collective-permute-start | bytes 9224 | tf_op jit(solution)/shard_map/ppermute | solution.py:30
  121.1 0.7 copy-start.2
  121.8 121.2 %all-gather.16.cloned.1.call-start = ((), (), s32[]{:S(2)}) async-start(), calls=%async_computation.4 | async-start | bytes 2359296 | tf_op jit(solution)/shard_map/all_gather | solution.py:142
  122.4 171.4 %all-gather.18.cloned.1.call-start = ((), (), s32[]{:S(2)}) async-start(), calls=%async_computation.5 | async-start | bytes 2359296 | tf_op jit(solution)/shard_map/all_gather | solution.py:198
  123.0 208.3 %reduce-scatter.2.cloned.1.call-start = ((), (), s32[]{:S(2)}) async-start(), calls=%async_computation.6 | async-start | bytes 3276800 | tf_op jit(solution)/shard_map/reduce_scatter | solution.py:201
  146.3 20.0 %collective-permute-start.5 = (bf16[3,256]{1,0:T(4,128)(2,1)S(1)}, bf16[3,256]{1,0:T(4,128)(2,1)S(1)}, u32[]{:S(2)}, u32[]{:S(2)}) collective-permute-start(bf16[3,256]{1,0:T(4,128)(2,1)S(1)} %slice.123), channel_id=1, source_target_pairs={{0,4},{4,8},{8,12},{12,16},{16,20},{20,24},{24,28},{1,5},{5,9},{9,... | collective-permute-start | bytes 4616 | tf_op jit(solution)/shard_map/ppermute | solution.py:30
  251.1 42.8 %copy-start.6 = (f32[640,512]{1,0:T(8,128)S(1)}, f32[640,512]{1,0:T(8,128)}, u32[]{:S(2)}) copy-start(f32[640,512]{1,0:T(8,128)} %get-tuple-element.310) | copy-start | bytes 3932164
Sparse Core Ops, SparseCore 0:
  9.5 42.9 all-gather.11
  54.6 47.7 all-gather.9
  104.6 38.7 all-gather.13
  145.4 47.8 all-gather.19
  195.2 47.7 all-gather.15
  244.9 48.8 all-gather.17
  298.6 32.6 reduce-scatter.1
